TPU v7x, 32 devices: a whole 2x2x4 slice. The times are simulated.
32 devices in a mesh: kv: 8 (over z, x), tp: 4 (over y, core).
Axes of the slice: x: 2, y: 2, z: 4, core: 2. Of those that a mesh axis runs over, the one named last changes fastest.
Arguments:
- tokens: bfloat16 [4096, 2048], P(('kv', 'tp')), may hold values from -6 to 6
- query_weight: bfloat16 [2048, 1024], P(None, 'tp'), may hold values from -0.125 to 0.125
- latent_weight: bfloat16 [2048, 256], replicated, may hold values from -0.125 to 0.125
- key_absorb: bfloat16 [8, 128, 256], P('tp'), may hold values from -0.5 to 0.5
- query_gain: bfloat16 [256], replicated, may hold values from 0.4 to 8
- latent_gain: bfloat16 [256], replicated, may hold values from 0.4 to 8
- value_absorb: bfloat16 [8, 256, 128], P('tp'), may hold values from -0.375 to 0.375
- head_gain: bfloat16 [8, 128], P('tp'), may hold values from 0.099609375 to 1.8984375
- out_weight: bfloat16 [1024, 2048], P('tp'), may hold values from -0.1875 to 0.1875
- chosen: int32 [64, 11], P('kv'), may hold values from 0 to 63, as said below
Outputs:
- mixed_out: bfloat16 [4096, 2048], P(('kv', 'tp'))
Inputs may be any that keep to these rules, and one draw needn't show every extreme that they name: `chosen`: entry 0 of row b is b; a row's entries are distinct. Entries 1 to 3 lie in the same aligned run of 8 block numbers as b, the other 7 in other runs. For each aligned run of 8 rows and each other aligned run of 8 block numbers, those rows together name at most one block of that run. Entries above the row's own number may occur and contribute nothing.
All inputs are finite; a program needn't handle non-finite values.
Results may differ from a plain program's by a relative error of at most 0.014.
The roundings to bfloat16 on the way count: a program that leaves them out, or rounds other values in their place, can miss the bound.
Values may be sent and summed in bfloat16 or wider, within the bound.
A program may use at most 64 MiB of HBM per device.

v0:
```python
import functools
import math

import jax
import jax.numpy as jnp
from jax import lax
from jax.experimental import pallas as pl
from jax.experimental.pallas import tpu as pltpu
from jax.sharding import PartitionSpec as P

epsilon = 1e-06
LOCAL = 4
SPLIT = 2
MESH = pl.DeviceIdType.MESH


def normalize(values, gain):
    return values * lax.rsqrt(jnp.mean(values * values, axis=-1, keepdims=True) + epsilon) * gain


def kernel(
    n_kv,
    tok_hbm,
    qw_hbm,
    lw_hbm,
    ka_hbm,
    qg_hbm,
    lg_hbm,
    va_hbm,
    hg_hbm,
    ow_hbm,
    ch_hbm,
    out,
    tok,
    qw,
    lw,
    ka,
    va,
    ow,
    qg_ref,
    lg_ref,
    hg_ref,
    ch_s,
    ch_v,
    lat,
    rem,
    stage,
    req,
    qabs,
    pre_out,
    pre_in,
    y_out,
    y_in,
    p_out,
    p_in,
    ld,
    tok_s,
    tok_r,
    lat_s,
    lat_r,
    req_s,
    req_r,
    blk_s,
    blk_r,
    share_s,
    share_r,
    red_s,
    red_r,
):
    kv = lax.axis_index("kv")
    t = lax.axis_index("tp")
    pair, core = t // 2, t % 2
    t1 = pair * 2 + (1 - core)
    t2 = (1 - pair) * 2 + core
    t3 = (1 - pair) * 2 + (1 - core)
    nblk, block, latent = lat.shape
    heads, head = ka.shape[0], ka.shape[1]
    rows = tok.shape[1]
    bpd = rows // block
    half = block // 2
    picks = ch_s.shape[1]
    f32, bf16 = jnp.float32, jnp.bfloat16

    loads = [
        pltpu.make_async_copy(src, dst, ld.at[i])
        for i, (src, dst) in enumerate(
            (
                (tok_hbm, tok.at[t]),
                (ch_hbm, ch_v),
                (lw_hbm, lw),
                (lg_hbm, lg_ref),
                (qw_hbm, qw),
                (ka_hbm, ka),
                (qg_hbm, qg_ref),
                (ch_hbm, ch_s),
                (va_hbm, va),
                (hg_hbm, hg_ref),
                (ow_hbm, ow),
            )
        )
    ]
    for load in loads:
        load.start()

    barrier = pltpu.get_barrier_semaphore()
    for peer in (t1, t2, t3):
        pl.semaphore_signal(barrier, inc=1, device_id={"tp": peer}, device_id_type=MESH)

    def greet(i, carry):
        pl.semaphore_signal(
            barrier, inc=1, device_id={"kv": (kv + i) % n_kv}, device_id_type=MESH
        )
        return carry

    lax.fori_loop(1, n_kv, greet, 0)
    loads[0].wait()
    loads[2].wait()
    loads[3].wait()
    own_latent = normalize(
        jnp.dot(tok[t], lw[...], preferred_element_type=f32),
        lg_ref[...].astype(f32).reshape(1, latent),
    ).astype(bf16)
    lat[pl.ds(t * bpd, bpd)] = own_latent.reshape(bpd, block, latent)
    loads[1].wait()
    pl.semaphore_wait(barrier, n_kv - 1 + 3)

    def send(src, dst, ss, rs, where):
        return pltpu.make_async_remote_copy(
            src_ref=src, dst_ref=dst, send_sem=ss, recv_sem=rs, device_id=where, device_id_type=MESH
        )

    def tok_part(r, c):
        return tok.at[r, pl.ds(c * block, block)]

    def tok_copy(kind, r, c, peer):
        return send(
            tok_part(r, c), tok_part(r, c), tok_s.at[kind, c], tok_r.at[kind, c], {"tp": peer}
        )

    far = [tok_copy(1, t, c, t2) for c in range(bpd)]
    near = [tok_copy(0, t, c, t1) for c in range(bpd)]
    relay = [tok_copy(2, t2, c, t1) for c in range(bpd)]
    own_lat = lat.at[pl.ds(t * bpd, bpd)]
    cross_lat = lat.at[pl.ds(t2 * bpd, bpd)]
    lat_copies = [
        send(own_lat, own_lat, lat_s.at[0], lat_r.at[0], {"tp": t2}),
        send(own_lat, own_lat, lat_s.at[1], lat_r.at[1], {"tp": t1}),
        send(cross_lat, cross_lat, lat_s.at[2], lat_r.at[2], {"tp": t1}),
    ]
    lat_copies[0].start()
    lat_copies[1].start()

    def req_copy(i, owner, peer):
        return send(ch_v, req.at[owner], req_s.at[i], req_r.at[i], {"kv": peer})

    def ask(i, carry):
        @pl.when(kv >= i)
        def _():
            req_copy(i, kv, kv - i).start()

        return carry

    lax.fori_loop(1, n_kv, ask, 0)

    for copy in far + near:
        copy.start()

    for load in loads[4:7]:
        load.wait()
    query_gain = qg_ref[...].astype(f32).reshape(1, latent)

    def project(r, start, count):
        queries = jnp.dot(
            tok[r, pl.ds(start, count), :], qw[...], preferred_element_type=f32
        ).astype(bf16)
        for h in range(heads):
            absorbed = jnp.dot(
                queries[:, h * head : (h + 1) * head], ka[h], preferred_element_type=f32
            )
            qabs[h, pl.ds(r * rows + start, count), :] = normalize(absorbed, query_gain).astype(bf16)

    lat_copies[0].wait_recv()
    lat_copies[2].start()
    lat_copies[1].wait_recv()
    lat_copies[2].wait_recv()

    def blk_copy(i, owner, peer):
        return send(stage.at[peer], rem.at[owner, core], blk_s.at[i], blk_r.at[i], {"kv": peer})

    def share_copy(i, owner):
        part = rem.at[owner, core]
        return send(part, part, share_s.at[i], share_r.at[i], {"tp": t1})

    def serve(step, carry):
        i = n_kv - step
        peer = kv + i

        @pl.when(peer < n_kv)
        def _():
            req_copy(i, peer, peer).wait_recv()
            wanted = req[peer]
            local = jnp.max(jnp.where(lax.div(wanted, nblk) == kv, lax.rem(wanted, nblk), 0))
            stage[peer] = jnp.where(core == 0, lat[local, :half], lat[local, half:])
            blk_copy(i, kv, peer).start()

        return carry

    lax.fori_loop(1, n_kv, serve, 0)
    rem[kv] = jnp.zeros((2, half, latent), bf16)

    project(t, 0, rows)
    for copy in near:
        copy.wait_recv()
    project(t1, 0, rows)

    def fetch(c):
        tok_copy(1, t2, c, t2).wait_recv()
        relay[c].start()
        project(t2, c * block, block)
        tok_copy(2, t3, c, t1).wait_recv()
        project(t3, c * block, block)

    fetch(0)

    def arrive(i, carry):
        @pl.when(kv >= i)
        def _():
            blk_copy(i, kv - i, kv - i).wait_recv()
            share_copy(i, kv - i).start()

        return carry

    lax.fori_loop(1, n_kv, arrive, 0)

    def arrive_shared(i, carry):
        @pl.when(kv >= i)
        def _():
            share_copy(i, kv - i).wait_recv()

        return carry

    lax.fori_loop(1, n_kv, arrive_shared, 0)
    for load in loads[7:]:
        load.wait()

    length = picks * block
    column = lax.broadcasted_iota(jnp.int32, (1, length), 1) // block
    lead = min(128, length)
    row_in = lax.rem(lax.broadcasted_iota(jnp.int32, (heads * block, lead), 0), block)
    col_in = lax.broadcasted_iota(jnp.int32, (heads * block, lead), 1)
    causal = jnp.where((col_in < block) & (col_in > row_in), -jnp.inf, 0.0).astype(f32)
    factor = latent ** (-0.5) * math.log2(math.e)
    head_gain = hg_ref[...].astype(f32)

    def attend(r, c):
        j = r * bpd + c
        b = kv * nblk + j
        q = qabs[:, pl.ds(j * block, block), :].reshape(heads * block, latent)
        parts = [lat[j]]
        bias = jnp.zeros((1, length), f32)
        for p in range(1, picks):
            pick = ch_s[j, p]
            seen = pick < b
            if p < LOCAL:
                parts.append(lat[jnp.where(seen, lax.rem(pick, nblk), j)])
            else:
                parts.append(rem[jnp.where(seen, lax.div(pick, nblk), kv)].reshape(block, latent))
            bias = jnp.where(column == p, jnp.where(seen, 0.0, -jnp.inf).astype(f32), bias)
        keys = jnp.concatenate(parts, axis=0)
        scores = (
            lax.dot_general(q, keys, (((1,), (1,)), ((), ())), preferred_element_type=f32) * factor
            + bias
        )
        scores = jnp.concatenate([scores[:, :lead] + causal, scores[:, lead:]], axis=1)
        top = jnp.max(scores, axis=-1, keepdims=True)
        weights = jnp.exp2(scores - top)
        total = jnp.sum(weights, axis=-1, keepdims=True)
        mixed = jnp.dot(weights.astype(bf16), keys, preferred_element_type=f32)
        mixed = (mixed / total).astype(bf16)
        outs = []
        for h in range(heads):
            values = jnp.dot(
                mixed[h * block : (h + 1) * block], va[h], preferred_element_type=f32
            )
            outs.append(normalize(values, head_gain[h : h + 1]).astype(bf16))
        return jnp.concatenate(outs, axis=1)

    def red_copy(kind, c, k, src, dst, peer):
        return send(
            src.at[c, k], dst.at[c, k], red_s.at[kind, c, k], red_r.at[kind, c, k], {"tp": peer}
        )

    piece = out.shape[1] // SPLIT
    cols = [slice(k * piece, (k + 1) * piece) for k in range(SPLIT)]
    reds = []

    def project_out(gathered, k):
        return jnp.dot(gathered, ow[:, cols[k]], preferred_element_type=f32).astype(bf16)

    def emit(kind, c, k, src, dst, peer, value):
        src[c, k] = value
        copy = red_copy(kind, c, k, src, dst, peer)
        copy.start()
        reds.append(copy)
        return copy

    for c in range(bpd):
        if c > 0:
            fetch(c)
        heads_out = attend(t3, c)
        pre = [emit(0, c, k, pre_out, pre_in, t1, project_out(heads_out, k)) for k in range(SPLIT)]
        heads_out = attend(t2, c)
        for k in range(SPLIT):
            mine = project_out(heads_out, k).astype(f32)
            pre[k].wait_recv()
            emit(1, c, k, y_out, y_in, t2, (mine + pre_in[c, k].astype(f32)).astype(bf16))
    for c in range(bpd):
        heads_out = attend(t1, c)
        for k in range(SPLIT):
            emit(2, c, k, p_out, p_in, t1, project_out(heads_out, k))
    for c in range(bpd):
        heads_out = attend(t, c)
        for k in range(SPLIT):
            out[pl.ds(c * block, block), cols[k]] = project_out(heads_out, k)
    for c in range(bpd):
        for k in range(SPLIT):
            red_copy(2, c, k, p_out, p_in, t1).wait_recv()
            red_copy(1, c, k, y_out, y_in, t2).wait_recv()
            place = pl.ds(c * block, block)
            out[place, cols[k]] = (
                out[place, cols[k]].astype(f32) + p_in[c, k].astype(f32) + y_in[c, k].astype(f32)
            ).astype(bf16)

    for copy in far + near + relay + lat_copies + reds:
        copy.wait_send()

    def finish(i, carry):
        @pl.when(kv >= i)
        def _():
            req_copy(i, kv, kv - i).wait_send()
            share_copy(i, kv - i).wait_send()

        @pl.when(kv + i < n_kv)
        def _():
            blk_copy(i, kv, kv + i).wait_send()

        return carry

    lax.fori_loop(1, n_kv, finish, 0)


def body(n_kv, n_tp, tokens, qw, lw, ka, qg, lg, va, hg, ow, chosen):
    rows, width = tokens.shape
    nblk = chosen.shape[0]
    block = rows * n_tp // nblk
    latent = lw.shape[1]
    bpd = rows // block
    bf16 = jnp.bfloat16
    hbm = pl.BlockSpec(memory_space=pltpu.HBM)
    vmem = pl.BlockSpec(memory_space=pltpu.VMEM)
    dma = pltpu.SemaphoreType.DMA
    piece = pltpu.VMEM((bpd, SPLIT, block, ow.shape[1] // SPLIT), bf16)
    arrays = [pltpu.with_memory_space_constraint(a, pltpu.HBM) for a in (tokens, qw, lw, ka, qg, lg, va, hg, ow, chosen)]
    return pl.pallas_call(
        functools.partial(kernel, n_kv),
        out_shape=jax.ShapeDtypeStruct((rows, ow.shape[1]), bf16),
        in_specs=[hbm] * 10,
        out_specs=vmem,
        scratch_shapes=[
            pltpu.VMEM((n_tp, rows, width), bf16),
            pltpu.VMEM(qw.shape, bf16),
            pltpu.VMEM(lw.shape, bf16),
            pltpu.VMEM(ka.shape, bf16),
            pltpu.VMEM(va.shape, bf16),
            pltpu.VMEM(ow.shape, bf16),
            pltpu.VMEM(qg.shape, bf16),
            pltpu.VMEM(lg.shape, bf16),
            pltpu.VMEM(hg.shape, bf16),
            pltpu.SMEM(chosen.shape, jnp.int32),
            pltpu.VMEM(chosen.shape, jnp.int32),
            pltpu.VMEM((nblk, block, latent), bf16),
            pltpu.VMEM((n_kv, 2, block // 2, latent), bf16),
            pltpu.VMEM((n_kv, block // 2, latent), bf16),
            pltpu.VMEM((n_kv,) + chosen.shape, jnp.int32),
            pltpu.VMEM((ka.shape[0], rows * n_tp, latent), bf16),
            piece,
            piece,
            piece,
            piece,
            piece,
            piece,
            dma((11,)),
            dma((3, bpd)),
            dma((3, bpd)),
            dma((3,)),
            dma((3,)),
            dma((n_kv,)),
            dma((n_kv,)),
            dma((n_kv,)),
            dma((n_kv,)),
            dma((n_kv,)),
            dma((n_kv,)),
            dma((3, bpd, SPLIT)),
            dma((3, bpd, SPLIT)),
        ],
        compiler_params=pltpu.CompilerParams(
            collective_id=0, has_side_effects=True, vmem_limit_bytes=50000000
        ),
    )(*arrays)


def solution(mesh):
    return jax.shard_map(
        functools.partial(body, mesh.shape["kv"], mesh.shape["tp"]),
        mesh=mesh,
        in_specs=(
            P(("kv", "tp"), None),
            P(None, "tp"),
            P(),
            P("tp", None, None),
            P(),
            P(),
            P("tp", None, None),
            P("tp", None),
            P("tp", None),
            P("kv", None),
        ),
        out_specs=P(("kv", "tp"), None),
        check_vma=False,
    )
```

profile of v0, /device:TPU:0, one launch (start us, length us, event | category | flops | bytes accessed | tf_op | source)
XLA Modules:
  0.0 35.2 jit_solution(4797402420264375732)
XLA Ops:
  0.0 34.4 %shard_map.100 = bf16[128,2048]{1,0:T(8,128)(2,1)S(1)} custom-call(bf16[128,2048]{1,0:T(8,128)(2,1)} %tok_hbm.1, bf16[2048,256]{1,0:T(8,128)(2,1)} %qw_hbm.1, bf16[2048,256]{1,0:T(8,128)(2,1)} %lw_hbm.1, bf16[2,128,256]{2,1,0:T(8,128)(2,1)} %ka_hbm.1, bf16[256]{0:T(256)(128)(2,1)} %qg_hbm.1, bf16[256]{0:T(256)(128)(2,1)} %lg_hbm.1, ...), custom_call_target="tpu_custom_call" | custom-call | tf_op jit(solution)/shard_map/pallas_call | solution.py:364
  34.4 0.8 %copy.12 = bf16[128,2048]{1,0:T(8,128)(2,1)} copy(bf16[128,2048]{1,0:T(8,128)(2,1)S(1)} %shard_map.100) | data formatting | bytes 1048576
where the time goes:
time: 35.3 us; the launch traced here: 35.2 us
  Pallas kernels  34.4 us (97%)
  local copies, waits for them, and re-layouts  0.8 us (2%)
    pallas_call x1, Pallas kernels, body(): pl.pallas_call(functools.partial(kernel, n_kv), out_shape=jax.ShapeDtypeS...  34.4 us
    unnamed x1, local copies, waits for them, and re-layouts  0.8 us

commit v1 on v0

--- a/solution.py
+++ b/solution.py
@@ -107,9 +107,12 @@
         pl.semaphore_signal(barrier, inc=1, device_id={"tp": peer}, device_id_type=MESH)
 
     def greet(i, carry):
-        pl.semaphore_signal(
-            barrier, inc=1, device_id={"kv": (kv + i) % n_kv}, device_id_type=MESH
-        )
+        @pl.when(kv + i < n_kv)
+        def _():
+            pl.semaphore_signal(
+                barrier, inc=1, device_id={"kv": kv + i}, device_id_type=MESH
+            )
+
         return carry
 
     lax.fori_loop(1, n_kv, greet, 0)
@@ -122,7 +125,7 @@
     ).astype(bf16)
     lat[pl.ds(t * bpd, bpd)] = own_latent.reshape(bpd, block, latent)
     loads[1].wait()
-    pl.semaphore_wait(barrier, n_kv - 1 + 3)
+    pl.semaphore_wait(barrier, kv + 3)
 
     def send(src, dst, ss, rs, where):
         return pltpu.make_async_remote_copy(
@@ -191,8 +194,7 @@
         part = rem.at[owner, core]
         return send(part, part, share_s.at[i], share_r.at[i], {"tp": t1})
 
-    def serve(step, carry):
-        i = n_kv - step
+    def serve(i, carry):
         peer = kv + i
 
         @pl.when(peer < n_kv)
@@ -205,13 +207,13 @@
 
         return carry
 
-    lax.fori_loop(1, n_kv, serve, 0)
     rem[kv] = jnp.zeros((2, half, latent), bf16)
 
     project(t, 0, rows)
     for copy in near:
         copy.wait_recv()
     project(t1, 0, rows)
+    lax.fori_loop(1, n_kv, serve, 0)
 
     def fetch(c):
         tok_copy(1, t2, c, t2).wait_recv()

time: 35.3 us -> 32.3 us (0.915)
  Pallas kernels: 34.4 us -> 31.3 us
    pallas_call x1, Pallas kernels: 34.4 us -> 31.3 us  [body(): pl.pallas_call(functools.partial(kernel, n_kv), out_shape=jax.ShapeDtypeS...]
where the time goes in v1:
time: 32.3 us; the launch traced here: 32.1 us
  Pallas kernels  31.3 us (97%)
  local copies, waits for them, and re-layouts  0.8 us (2%)
    pallas_call x1, Pallas kernels, body(): pl.pallas_call(functools.partial(kernel, n_kv), out_shape=jax.ShapeDtypeS...  31.3 us
    unnamed x1, local copies, waits for them, and re-layouts  0.8 us

profile of v1, /device:TPU:0, one launch (start us, length us, event | category | flops | bytes accessed | tf_op | source)
XLA Modules:
  0.0 32.1 jit_solution(4336049497358289167)
XLA Ops:
  0.0 31.3 %shard_map.100 = bf16[128,2048]{1,0:T(8,128)(2,1)S(1)} custom-call(bf16[128,2048]{1,0:T(8,128)(2,1)} %tok_hbm.1, bf16[2048,256]{1,0:T(8,128)(2,1)} %qw_hbm.1, bf16[2048,256]{1,0:T(8,128)(2,1)} %lw_hbm.1, bf16[2,128,256]{2,1,0:T(8,128)(2,1)} %ka_hbm.1, bf16[256]{0:T(256)(128)(2,1)} %qg_hbm.1, bf16[256]{0:T(256)(128)(2,1)} %lg_hbm.1, ...), custom_call_target="tpu_custom_call" | custom-call | tf_op jit(solution)/shard_map/pallas_call | solution.py:366
  31.3 0.8 %copy.12 = bf16[128,2048]{1,0:T(8,128)(2,1)} copy(bf16[128,2048]{1,0:T(8,128)(2,1)S(1)} %shard_map.100) | data formatting | bytes 1048576

commit v2 on v1

--- a/solution.py
+++ b/solution.py
@@ -11,6 +11,7 @@
 epsilon = 1e-06
 LOCAL = 4
 SPLIT = 2
+EARLY = 16
 MESH = pl.DeviceIdType.MESH
 
 
@@ -56,6 +57,8 @@
     ld,
     tok_s,
     tok_r,
+    early_s,
+    early_r,
     lat_s,
     lat_r,
     req_s,
@@ -116,6 +119,15 @@
         return carry
 
     lax.fori_loop(1, n_kv, greet, 0)
+    def send(src, dst, ss, rs, where):
+        return pltpu.make_async_remote_copy(
+            src_ref=src, dst_ref=dst, send_sem=ss, recv_sem=rs, device_id=where, device_id_type=MESH
+        )
+
+    def early_copy(r):
+        part = tok.at[r, pl.ds(0, EARLY)]
+        return send(part, part, early_s.at[0], early_r.at[0], {"tp": t2})
+
     loads[0].wait()
     loads[2].wait()
     loads[3].wait()
@@ -124,20 +136,28 @@
         lg_ref[...].astype(f32).reshape(1, latent),
     ).astype(bf16)
     lat[pl.ds(t * bpd, bpd)] = own_latent.reshape(bpd, block, latent)
+    pl.semaphore_wait(barrier, kv + 3)
     loads[1].wait()
-    pl.semaphore_wait(barrier, kv + 3)
-
-    def send(src, dst, ss, rs, where):
-        return pltpu.make_async_remote_copy(
-            src_ref=src, dst_ref=dst, send_sem=ss, recv_sem=rs, device_id=where, device_id_type=MESH
-        )
-
-    def tok_part(r, c):
-        return tok.at[r, pl.ds(c * block, block)]
+
+    def req_copy(i, owner, peer):
+        return send(ch_v, req.at[owner], req_s.at[i], req_r.at[i], {"kv": peer})
+
+    def ask(i, carry):
+        @pl.when(kv >= i)
+        def _():
+            req_copy(i, kv, kv - i).start()
+
+        return carry
+
+    lax.fori_loop(1, n_kv, ask, 0)
+
+    def tok_part(r, c, kind):
+        start = EARLY if kind == 1 and c == 0 else c * block
+        return tok.at[r, pl.ds(start, (c + 1) * block - start)]
 
     def tok_copy(kind, r, c, peer):
         return send(
-            tok_part(r, c), tok_part(r, c), tok_s.at[kind, c], tok_r.at[kind, c], {"tp": peer}
+            tok_part(r, c, kind), tok_part(r, c, kind), tok_s.at[kind, c], tok_r.at[kind, c], {"tp": peer}
         )
 
     far = [tok_copy(1, t, c, t2) for c in range(bpd)]
@@ -152,18 +172,7 @@
     ]
     lat_copies[0].start()
     lat_copies[1].start()
-
-    def req_copy(i, owner, peer):
-        return send(ch_v, req.at[owner], req_s.at[i], req_r.at[i], {"kv": peer})
-
-    def ask(i, carry):
-        @pl.when(kv >= i)
-        def _():
-            req_copy(i, kv, kv - i).start()
-
-        return carry
-
-    lax.fori_loop(1, n_kv, ask, 0)
+    early_copy(t).start()
 
     for copy in far + near:
         copy.start()
@@ -215,15 +224,16 @@
     project(t1, 0, rows)
     lax.fori_loop(1, n_kv, serve, 0)
 
-    def fetch(c):
+    def fetch_cross(c):
+        if c == 0:
+            early_copy(t2).wait_recv()
         tok_copy(1, t2, c, t2).wait_recv()
         relay[c].start()
-        project(t2, c * block, block)
+
+    def fetch_relayed(c):
         tok_copy(2, t3, c, t1).wait_recv()
         project(t3, c * block, block)
 
-    fetch(0)
-
     def arrive(i, carry):
         @pl.when(kv >= i)
         def _():
@@ -232,7 +242,12 @@
 
         return carry
 
-    lax.fori_loop(1, n_kv, arrive, 0)
+    late = kv // ((n_kv + 1) // 2)
+    ready = 1 + (n_kv - 1) * (1 - late)
+    lax.fori_loop(1, ready, arrive, 0)
+    fetch_cross(0)
+    lax.fori_loop(ready, n_kv, arrive, 0)
+    project(t2, 0, block)
 
     def arrive_shared(i, carry):
         @pl.when(kv >= i)
@@ -308,14 +323,16 @@
 
     for c in range(bpd):
         if c > 0:
-            fetch(c)
+            fetch_cross(c)
+            project(t2, c * block, block)
+        heads_out = attend(t2, c)
+        pre = [emit(0, c, k, pre_out, pre_in, t1, project_out(heads_out, k)) for k in range(SPLIT)]
+        fetch_relayed(c)
         heads_out = attend(t3, c)
-        pre = [emit(0, c, k, pre_out, pre_in, t1, project_out(heads_out, k)) for k in range(SPLIT)]
-        heads_out = attend(t2, c)
         for k in range(SPLIT):
-            mine = project_out(heads_out, k).astype(f32)
+            theirs = project_out(heads_out, k).astype(f32)
             pre[k].wait_recv()
-            emit(1, c, k, y_out, y_in, t2, (mine + pre_in[c, k].astype(f32)).astype(bf16))
+            emit(1, c, k, y_out, y_in, t3, (theirs + pre_in[c, k].astype(f32)).astype(bf16))
     for c in range(bpd):
         heads_out = attend(t1, c)
         for k in range(SPLIT):
@@ -327,12 +344,13 @@
     for c in range(bpd):
         for k in range(SPLIT):
             red_copy(2, c, k, p_out, p_in, t1).wait_recv()
-            red_copy(1, c, k, y_out, y_in, t2).wait_recv()
+            red_copy(1, c, k, y_out, y_in, t3).wait_recv()
             place = pl.ds(c * block, block)
             out[place, cols[k]] = (
                 out[place, cols[k]].astype(f32) + p_in[c, k].astype(f32) + y_in[c, k].astype(f32)
             ).astype(bf16)
 
+    early_copy(t).wait_send()
     for copy in far + near + relay + lat_copies + reds:
         copy.wait_send()
 
@@ -394,6 +412,8 @@
             dma((11,)),
             dma((3, bpd)),
             dma((3, bpd)),
+            dma((1,)),
+            dma((1,)),
             dma((3,)),
             dma((3,)),
             dma((n_kv,)),

time: 32.3 us -> 31.6 us (0.978)
  the two profiles are of different devices: /device:TPU:0 before, /device:TPU:25 now
where the time goes in v2:
time: 31.6 us; the launch traced here: 31.4 us
  Pallas kernels  30.6 us (97%)
  local copies, waits for them, and re-layouts  0.8 us (3%)
    pallas_call x1, Pallas kernels, body(): pl.pallas_call(functools.partial(kernel, n_kv), out_shape=jax.ShapeDtypeS...  30.6 us
    unnamed x1, local copies, waits for them, and re-layouts  0.8 us

profile of v2, /device:TPU:25, one launch (start us, length us, event | category | flops | bytes accessed | tf_op | source)
XLA Modules:
  0.0 31.4 jit_solution(1763081856419329615)
XLA Ops:
  0.0 30.6 %shard_map.100 = bf16[128,2048]{1,0:T(8,128)(2,1)S(1)} custom-call(bf16[128,2048]{1,0:T(8,128)(2,1)} %tok_hbm.1, bf16[2048,256]{1,0:T(8,128)(2,1)} %qw_hbm.1, bf16[2048,256]{1,0:T(8,128)(2,1)} %lw_hbm.1, bf16[2,128,256]{2,1,0:T(8,128)(2,1)} %ka_hbm.1, bf16[256]{0:T(256)(128)(2,1)} %qg_hbm.1, bf16[256]{0:T(256)(128)(2,1)} %lg_hbm.1, ...), custom_call_target="tpu_custom_call" | custom-call | tf_op jit(solution)/shard_map/pallas_call | solution.py:384
  30.6 0.8 %copy.12 = bf16[128,2048]{1,0:T(8,128)(2,1)} copy(bf16[128,2048]{1,0:T(8,128)(2,1)S(1)} %shard_map.100) | data formatting | bytes 1048576
